TPU v7x, 32 devices: a whole 2x2x4 slice. The times are simulated.
32 devices in a mesh: sp: 8 (over z, y), tp: 4 (over x, core).
Axes of the slice: x: 2, y: 2, z: 4, core: 2. Of those that a mesh axis runs over, the one named last changes fastest.
Arguments:
- queries: bfloat16 [3072, 2048], P('sp', 'tp'), may hold values from -6 to 6
- keys: bfloat16 [3072, 2048], P('sp', 'tp'), may hold values from -6 to 6
- values: bfloat16 [3072, 2048], P('sp', 'tp'), may hold values from -6 to 6
- gates: bfloat16 [3072, 2048], P('sp', 'tp'), may hold values from -8 to 8
- decay_pre: float32 [32, 3072], P('tp', 'sp'), may hold values from -18 to 3
- beta_pre: float32 [32, 3072], P('tp', 'sp'), may hold values from -10 to 3
- out_gain: float32 [64], replicated, may hold values from 0.1 to 1.9
- w_out: bfloat16 [2048, 2048], P('tp'), may hold values from -0.125 to 0.125
- stream: bfloat16 [3072, 2048], P(('sp', 'tp')), may hold values from -6 to 6
- norm_gain: float32 [2048], replicated, may hold values from 0.1 to 1.9
- w_gate: bfloat16 [2048, 5632], P('sp', 'tp'), may hold values from -0.125 to 0.125
- w_up: bfloat16 [2048, 5632], P('sp', 'tp'), may hold values from -0.125 to 0.125
- w_down: bfloat16 [5632, 2048], P('tp', 'sp'), may hold values from -0.078125 to 0.078125
Outputs:
- updated: bfloat16 [3072, 2048], P(('sp', 'tp'))
All inputs are finite; a program needn't handle non-finite values.
Results may differ from a plain program's by a relative error of at most 0.019.
Values may be sent and summed in bfloat16 or wider, within the bound.
A program may use at most 128 MiB of HBM per device.

v0:
```python
import jax
import jax.numpy as jnp
from jax import lax
from jax.sharding import PartitionSpec as P

HEAD_DIM = 64
BLOCK = 64
EPSILON = 1e-06
EXACT_PRECISION = lax.Precision.HIGHEST


def prefix(x, axis, combine, identity):
    size, index = (lax.axis_size(axis), lax.axis_index(axis))
    everything = jax.tree.map(
        lambda part, kind: lax.all_gather(part.astype(kind), axis), x, (jnp.bfloat16, jnp.bfloat16)
    )
    start = jax.tree.map(
        lambda part, zero: jnp.broadcast_to(jnp.asarray(zero, part.dtype), part.shape), x, identity
    )

    def hop(k, before):
        reached = k < index
        new = combine(
            before, jax.tree.map(lambda part, own: part[k].astype(own.dtype), everything, x)
        )
        return jax.tree.map(lambda a, b: jnp.where(reached, a, b), new, before)

    return lax.fori_loop(0, size, hop, start)


def unit_lower_inverse(lower_mat):
    span_len = lower_mat.shape[-1]
    identity = jnp.eye(span_len, dtype=jnp.float32)
    power = -lower_mat
    inverse = identity + power
    steps = 1
    while 1 << steps < span_len:
        power = jnp.einsum("...ij,...jk->...ik", power, power, precision=EXACT_PRECISION)
        inverse = jnp.einsum(
            "...ij,...jk->...ik", inverse, identity + power, precision=EXACT_PRECISION
        )
        steps = steps + 1
    return inverse


def prepare(queries, keys, values, beta_pre, decay_pre):
    length = queries.shape[0]
    heads = queries.shape[1] // HEAD_DIM

    def split_heads(arr):
        return arr.astype(jnp.float32).reshape(length, heads, HEAD_DIM)

    query_unit = jax.nn.silu(split_heads(queries))
    query_unit = query_unit * lax.rsqrt(
        jnp.sum(query_unit * query_unit, axis=-1, keepdims=True) + EPSILON
    )
    query_unit = (query_unit * HEAD_DIM ** (-0.5)).astype(jnp.bfloat16)
    key_unit = jax.nn.silu(split_heads(keys))
    key_unit = (
        key_unit * lax.rsqrt(jnp.sum(key_unit * key_unit, axis=-1, keepdims=True) + EPSILON)
    ).astype(jnp.bfloat16)
    value_act = jax.nn.silu(split_heads(values))
    strength = jax.nn.sigmoid(beta_pre)
    log_decay = -jax.nn.softplus(decay_pre)
    nblocks = length // BLOCK

    def blocked(arr):
        return arr.reshape(nblocks, BLOCK, heads, HEAD_DIM).transpose(0, 2, 1, 3)

    def blocked_rates(arr):
        return arr.reshape(heads, nblocks, BLOCK).transpose(1, 0, 2)

    return (
        blocked(query_unit),
        blocked(key_unit),
        blocked(value_act),
        blocked_rates(strength),
        blocked_rates(log_decay),
    )


def block_terms(query_blk, key_blk, value_blk, strength_blk, decay_blk):
    span_len = query_blk.shape[-2]
    query_f = query_blk.astype(jnp.float32)
    key_f = key_blk.astype(jnp.float32)
    cumulative = jnp.cumsum(decay_blk, axis=-1)
    row_ids = jnp.arange(span_len)[:, None]
    col_ids = jnp.arange(span_len)[None, :]
    inclusive = row_ids >= col_ids
    strict = row_ids > col_ids
    decay_mat = jnp.exp(
        jnp.where(inclusive, cumulative[..., :, None] - cumulative[..., None, :], -jnp.inf)
    )
    key_inner = jnp.einsum(
        "...id,...jd->...ij", key_blk, key_blk, preferred_element_type=jnp.float32
    )
    lower_mat = jnp.where(strict, strength_blk[..., :, None] * key_inner * decay_mat, 0.0)
    key_strong = key_f * strength_blk[..., None]
    right_side = jnp.concatenate(
        [value_blk * strength_blk[..., None], key_strong * jnp.exp(cumulative)[..., None]], axis=-1
    )
    solved = jnp.einsum(
        "...ij,...jk->...ik", unit_lower_inverse(lower_mat), right_side, precision=EXACT_PRECISION
    )
    width = value_blk.shape[-1]
    update_values = solved[..., :width]
    update_keys = solved[..., width:]
    query_inner = jnp.einsum(
        "...id,...jd->...ij", query_blk, key_blk, preferred_element_type=jnp.float32
    )
    inside_span = jnp.where(inclusive, query_inner * decay_mat, 0.0)
    final_decay = cumulative[..., -1:]
    key_attenuated = key_f * jnp.exp(final_decay - cumulative)[..., None]
    query_attenuated = query_f * jnp.exp(cumulative)[..., None]
    return (update_values, update_keys, inside_span, query_attenuated, key_attenuated, final_decay)


def advance(matrix_state, terms):
    update_values, update_keys, inside_span, query_attenuated, key_attenuated, final_decay = terms
    value_corrected = update_values - jnp.einsum(
        "jod,jdg->jog", update_keys, matrix_state, precision=EXACT_PRECISION
    )
    output_result = jnp.einsum(
        "jod,jdg->jog", query_attenuated, matrix_state, precision=EXACT_PRECISION
    ) + jnp.einsum("oyn,onk->oyk", inside_span, value_corrected, precision=EXACT_PRECISION)
    matrix_state = matrix_state * jnp.exp(final_decay)[..., None] + jnp.einsum(
        "lyq,lyf->lqf", key_attenuated, value_corrected, precision=EXACT_PRECISION
    )
    return (matrix_state, output_result)


def compose(carry, items):
    trans_mat, offset_mat = carry
    update_keys, update_values, key_attenuated, final_decay = items
    heads = update_keys.shape[0]
    identity = jnp.broadcast_to(jnp.eye(HEAD_DIM, dtype=jnp.float32), (heads, HEAD_DIM, HEAD_DIM))
    step_trans = jnp.exp(final_decay)[..., None] * identity - jnp.einsum(
        "hck,hcl->hkl", key_attenuated, update_keys, precision=EXACT_PRECISION
    )
    stride_displacement = jnp.einsum(
        "lyq,lyf->lqf", key_attenuated, update_values, precision=EXACT_PRECISION
    )
    new_trans = jnp.einsum("hkl,hlm->hkm", step_trans, trans_mat, precision=EXACT_PRECISION)
    new_offset = (
        jnp.einsum("hkl,hlm->hkm", step_trans, offset_mat, precision=EXACT_PRECISION)
        + stride_displacement
    )
    return ((new_trans, new_offset), None)


def chain(earlier, later):
    joined_trans = jnp.einsum("hkl,hlm->hkm", later[0], earlier[0], precision=EXACT_PRECISION)
    joined_offset = (
        jnp.einsum("hkl,hlm->hkm", later[0], earlier[1], precision=EXACT_PRECISION) + later[1]
    )
    return (joined_trans, joined_offset)


def finish(outputs, gates, out_gain):
    length = gates.shape[0]
    heads = gates.shape[1] // HEAD_DIM
    heads_out = outputs.transpose(0, 2, 1, 3).reshape(length, heads, HEAD_DIM)
    heads_out = heads_out * lax.rsqrt(
        jnp.mean(heads_out * heads_out, axis=-1, keepdims=True) + EPSILON
    )
    heads_out = heads_out * out_gain
    gated = heads_out * jax.nn.silu(gates.astype(jnp.float32).reshape(length, heads, HEAD_DIM))
    return gated.reshape(length, heads * HEAD_DIM).astype(jnp.bfloat16)


def per_device(
    queries,
    keys,
    values,
    gates,
    decay_pre,
    beta_pre,
    out_gain,
    w_out,
    stream,
    norm_gain,
    w_gate,
    w_up,
    w_down,
):
    blocks = prepare(queries, keys, values, beta_pre, decay_pre)
    terms = block_terms(*blocks)
    update_values, update_keys, inside_span, query_attenuated, key_attenuated, final_decay = terms
    heads = update_keys.shape[1]
    identity = jnp.broadcast_to(jnp.eye(HEAD_DIM, dtype=jnp.float32), (heads, HEAD_DIM, HEAD_DIM))
    zero_state = jnp.zeros((heads, HEAD_DIM, HEAD_DIM), jnp.float32)
    (trans_mat, offset_mat), _ = lax.scan(
        compose, (identity, zero_state), (update_keys, update_values, key_attenuated, final_decay)
    )
    earlier_part = prefix((trans_mat, offset_mat), "sp", chain, (identity, zero_state))
    _, outputs = lax.scan(advance, earlier_part[1], terms)
    mixed_heads = finish(outputs, gates, out_gain)
    head_block = lax.all_to_all(mixed_heads, "tp", split_axis=0, concat_axis=1, tiled=True)
    out_whole = lax.all_gather(w_out, "tp", axis=0, tiled=True)
    projected = jnp.dot(head_block, out_whole, preferred_element_type=jnp.float32)
    middle = (stream.astype(jnp.float32) + projected).astype(jnp.bfloat16)
    middle_f = middle.astype(jnp.float32)
    normed = middle_f * lax.rsqrt(jnp.mean(middle_f * middle_f, axis=-1, keepdims=True) + EPSILON)
    normed = (normed * norm_gain).astype(jnp.bfloat16)
    span_rows = lax.all_gather(normed, "tp", axis=0, tiled=True)
    gate_hidden = jnp.dot(
        span_rows,
        lax.all_gather(w_gate, "sp", axis=0, tiled=True),
        preferred_element_type=jnp.float32,
    )
    up_hidden = jnp.dot(
        span_rows,
        lax.all_gather(w_up, "sp", axis=0, tiled=True),
        preferred_element_type=jnp.float32,
    )
    hidden = (jax.nn.silu(gate_hidden) * up_hidden).astype(jnp.bfloat16)
    channel_term = jnp.dot(
        hidden, lax.all_gather(w_down, "sp", axis=1, tiled=True), preferred_element_type=jnp.float32
    )
    channel_sum = lax.psum_scatter(
        channel_term.astype(jnp.bfloat16), "tp", scatter_dimension=0, tiled=True
    ).astype(jnp.float32)
    return (middle_f + 0.5 * channel_sum).astype(jnp.bfloat16)


def solution(mesh):
    return jax.shard_map(
        per_device,
        mesh=mesh,
        in_specs=(
            P("sp", "tp"),
            P("sp", "tp"),
            P("sp", "tp"),
            P("sp", "tp"),
            P("tp", "sp"),
            P("tp", "sp"),
            P(),
            P("tp", None),
            P(("sp", "tp"), None),
            P(),
            P("sp", "tp"),
            P("sp", "tp"),
            P("tp", "sp"),
        ),
        out_specs=P(("sp", "tp"), None),
        check_vma=False,
    )
```

profile of v0, /device:TPU:0, one launch (start us, length us, event | category | flops | bytes accessed | tf_op | source)
XLA Modules:
  0.0 467.6 jit_solution(12672921094007981784)
XLA Ops:
  8.3 1.8 reshape.144
  13.1 2.7 copy.76
  16.0 1.6 copy.66
  17.8 1.5 reshape.139
  19.4 5.9 %fusion.46 = (f32[6,8,64,64]{3,2,1,0:T(8,128)S(1)}, bf16[6,64,8,64]{3,1,2,0:T(8,128)(2,1)S(1)}, f32[6,8,64,64]{3,2,1,0:T(8,128)}, f32[6,8,64,64]{3,2,1,0:T(8,128)S(1)}) fusion(f32[6,8,64]{2,1,0:T(8,128)S(1)} %get-tuple-element.343, f32[6,8,64]{2,1,0:T(8,128)S(1)} %copy.68, f32[6,64,8]{1,2,0:T(8,128)S(1)} %copy.67, f32[6,64,8,64]{3,1,2,0:T(8,128)} %copy.66, ...), kind=kLoop, calls=%fused_computation.60 | loop fusion | flops 4521984 | bytes 5160960 | tf_op jit(solution)/shard_map/mul | solution.py:100
  25.3 2.7 multiply_select_fusion
  28.9 1.8 fusion.81
  30.7 1.8 fusion.82
  32.5 1.8 fusion.59
  34.3 1.8 fusion.83
  36.1 1.7 fusion.57
  37.8 1.8 fusion.84
  39.5 1.9 fusion.55
  41.5 1.8 fusion.85
  43.2 1.8 fusion.53
  45.0 1.8 fusion.51
  46.8 1.9 fusion.47
  48.6 2.2 fusion.79
  50.8 1.6 convert_multiply_fusion.1
  52.5 1.9 copy.72
  54.5 21.4 %while.43 = (s32[]{:T(128)}, f32[8,64,64]{2,1,0:T(8,128)S(1)}, f32[8,64,64]{2,1,0:T(8,128)S(1)}, f32[6,8,1]{1,2,0:T(1,128)S(1)}, f32[6,8,64,64]{2,3,1,0:T(8,128)...) while((s32[]{:T(128)}, f32[8,64,64]{2,1,0:T(8,128)S(1)}, ...), condition=%wide.region_3.4_spmd.clone.clone, body=%wide.region_2.3_spmd.clone.sunk.clone | while | flops 100802560 | bytes 2673307 | solution.py:192
  54.5 1.3 convolution_subtract_fusion.7
  56.3 1.3 convolution_add_fusion.10
  58.1 1.3 convolution_subtract_fusion.7
  59.8 1.3 convolution_add_fusion.10
  61.7 1.3 convolution_subtract_fusion.7
  63.4 1.4 convolution_add_fusion.10
  65.2 1.3 convolution_subtract_fusion.7
  67.0 1.3 convolution_add_fusion.10
  68.8 1.4 convolution_subtract_fusion.7
  70.6 1.3 convolution_add_fusion.10
  72.4 1.3 convolution_subtract_fusion.7
  74.1 1.3 convolution_add_fusion.10
  75.9 41.2 %all-gather = bf16[64,64,64]{2,1,0:T(8,128)(2,1)} all-gather(bf16[8,64,64]{2,1,0:T(8,128)(2,1)S(1)} %convert_element_type.98), channel_id=2, replica_groups=mesh['sp'=8,'tp'=4] {'sp'}, dimensions={0}, use_global_device_ids=true | all-gather | bytes 589824 | tf_op jit(solution)/shard_map/all_gather | solution.py:15
  117.2 38.8 %all-gather.1 = bf16[64,64,64]{2,1,0:T(8,128)(2,1)} all-gather(bf16[8,64,64]{2,1,0:T(8,128)(2,1)S(1)} %convert_element_type.99), channel_id=3, replica_groups=mesh['sp'=8,'tp'=4] {'sp'}, dimensions={0}, use_global_device_ids=true | all-gather | bytes 589824 | tf_op jit(solution)/shard_map/all_gather | solution.py:15
  156.0 10.7 %while.44 = (s32[]{:T(128)}, f32[8,64,64]{2,1,0:T(8,128)S(1)}, s32[]{:T(128)}, bf16[8,8,64,64]{3,2,1,0:T(8,128)(2,1)}, bf16[8,8,64,64]{3,2,1,0:T(8,128)(2,1)}) while((s32[]{:T(128)}, f32[8,64,64]{2,1,0:T(8,128)S(1)}, s32[]{:T(128)}, bf16[8,8,64,64]{3,2,1,0:T(8,128)(2,1)}, bf16[8,8,64,64]{3,2,1,0:T(8,128)(2,1)}) %tuple.113), condition=%wide.region_5.6_spmd.clone.clone, body=%wide.region_4.5_spmd.clone.sunk.clone | while | flops 25329668 | bytes 1182287 | solution.py:28
  166.7 27.7 %while.42 = (s32[]{:T(128)}, f32[8,64,64]{2,1,0:T(8,128)S(1)}, f32[6,8,64,64]{3,2,1,0:T(8,128)S(1)}, f32[6,8,1]{1,2,0:T(1,128)S(1)}, f32[6,8,64,64]{2,3,1,0:T(8,...) while((s32[]{:T(128)}, f32[8,64,64]{2,1,0:T(8,128)S(1)}, ...), condition=%wide.region_8.9_spmd.clone, body=%wide.region_7.8_spmd.sunk.clone | while | flops 100794368 | bytes 3280037 | solution.py:196
  166.7 1.4 convolution_subtract_fusion.6
  168.1 1.3 fusion.177
  169.5 1.3 fusion.178
  171.3 1.4 convolution_subtract_fusion.6
  172.8 1.3 fusion.177
  174.1 1.3 fusion.178
  176.0 1.4 convolution_subtract_fusion.6
  177.4 1.3 fusion.177
  178.7 1.3 fusion.178
  180.6 1.4 convolution_subtract_fusion.6
  182.0 1.3 fusion.177
  183.4 1.3 fusion.178
  185.2 1.4 convolution_subtract_fusion.6
  186.6 1.3 fusion.177
  188.0 1.3 fusion.178
  189.8 1.4 convolution_subtract_fusion.6
  191.3 1.3 fusion.177
  192.6 1.3 fusion.178
  198.7 9.8 %all_to_all.19 = bf16[4,96,512]{2,1,0:T(8,128)(2,1)S(1)} all-to-all(bf16[4,96,512]{2,1,0:T(8,128)(2,1)S(1)} %bitcast.177), channel_id=1, replica_groups=mesh['sp'=8,'tp'=4] {'tp'}, dimensions={0} | all-to-all | bytes 786432 | tf_op jit(solution)/shard_map/all_to_all | solution.py:198
  208.6 5.0 %multiply_reduce_fusion.1 = (f32[96]{0:T(128)S(1)}, f32[96,2048]{1,0:T(8,128)S(1)}) fusion(bf16[96,2048]{1,0:T(8,128)(2,1)S(1)} %bitcast.173, bf16[2048,2048]{1,0:T(8,128)(2,1)} %all-gather.8.cloned.1.call-done, bf16[96,2048]{1,0:T(8,128)(2,1)S(1)} %copy-done.7), kind=kOutput, calls=%fused_computation.95 | convolution fusion | flops 806485888 | bytes 9961856 | tf_op jit(solution)/shard_map/dot_general | solution.py:200
  215.7 17.8 %all-gather.10.cloned.1.call-done = bf16[384,2048]{1,0:T(8,128)(2,1)} async-done(((bf16[96,2048]{1,0:T(8,128)(2,1)}), bf16[384,2048]{1,0:T(8,128)(2,1)}) %all-gather.10.cloned.1.call-update) | async-done | bytes 1572880 | tf_op jit(solution)/shard_map/all_gather | solution.py:205
  233.5 7.2 %fusion.86 = f32[384,1408]{1,0:T(8,128)} fusion(bf16[384,2048]{1,0:T(8,128)(2,1)} %all-gather.10.cloned.1.call-done, bf16[2048,1408]{1,0:T(8,128)(2,1)} %all-gather.12.cloned.1.call-done), kind=kOutput, calls=%fused_computation.126 | convolution fusion | flops 2214592512 | bytes 9502720 | tf_op jit(solution)/shard_map/dot_general | solution.py:206
  240.7 87.2 %all-gather.14.cloned.1.call-done = bf16[2048,1408]{1,0:T(8,128)(2,1)} async-done(((bf16[256,1408]{1,0:T(8,128)(2,1)}), bf16[2048,1408]{1,0:T(8,128)(2,1)}) %all-gather.14.cloned.1.call-update) | async-done | bytes 5767184 | tf_op jit(solution)/shard_map/all_gather | solution.py:213
  327.9 93.2 %all-gather.16.cloned.1.call-done = bf16[1408,2048]{1,0:T(8,128)(2,1)} async-done(((bf16[1408,256]{1,0:T(8,128)(2,1)}), bf16[1408,2048]{1,0:T(8,128)(2,1)}) %all-gather.16.cloned.1.call-update) | async-done | bytes 5767184 | tf_op jit(solution)/shard_map/all_gather | solution.py:218
  421.1 11.2 %convolution_convert_fusion = bf16[384,2048]{1,0:T(8,128)(2,1)} fusion(bf16[1408,2048]{1,0:T(8,128)(2,1)} %all-gather.16.cloned.1.call-done, bf16[384,2048]{1,0:T(8,128)(2,1)S(1)} %copy-done.12, bf16[2048,1408]{1,0:T(8,128)(2,1)} %all-gather.14.cloned.1.call-done, f32[384,1408]{1,0:T(8,128)} %fusion.86), kind=kOutput, calls=%fused_computation.54 | convolution fusion | flops 4433215488 | bytes 16842752 | tf_op jit(solution)/shard_map/dot_general | solution.py:217
  432.3 26.4 %reduce-scatter.2.cloned.1.call-done = bf16[96,2048]{1,0:T(8,128)(2,1)} async-done(((bf16[384,2048]{1,0:T(8,128)(2,1)}), bf16[96,2048]{1,0:T(8,128)(2,1)}) %reduce-scatter.2.cloned.1.call-update) | async-done | bytes 393232 | tf_op jit(solution)/shard_map/reduce_scatter | solution.py:220
  458.7 1.8 add_convert_fusion
  (142 shorter events, 30.3 us)
Async XLA Ops:
  6.5 1.5 copy-start.3
  6.5 202.0 %all-gather.8.cloned.1.call-start = ((), (), s32[]{:S(2)}) async-start(), calls=%async_computation.2 | async-start | bytes 10485760 | tf_op jit(solution)/shard_map/all_gather | solution.py:199
  7.3 208.4 %all-gather.12.cloned.1.call-start = ((), (), s32[]{:S(2)}) async-start(), calls=%async_computation.4 | async-start | bytes 6488064 | tf_op jit(solution)/shard_map/all_gather | solution.py:208
  8.0 225.5 %all-gather.10.cloned.1.call-start = ((), (), s32[]{:S(2)}) async-start(), calls=%async_computation.3 | async-start | bytes 1966080 | tf_op jit(solution)/shard_map/all_gather | solution.py:205
  8.3 2.1 copy-start.4
  10.6 0.8 copy-start.8
  16.0 1.7 copy-start.9
  16.0 1.8 copy-start.5
  17.6 1.8 copy-start
  117.2 49.5 %copy-start.1 = (f32[6,8,64,64]{3,2,1,0:T(8,128)S(1)}, f32[6,8,64,64]{3,2,1,0:T(8,128)}, u32[]{:S(2)}) copy-start(f32[6,8,64,64]{3,2,1,0:T(8,128)} %custom-call.2) | copy-start | bytes 2359300
  197.1 0.7 copy-start.11
  197.1 1.1 copy-start.2
  197.1 1.2 copy-start.6
  198.4 10.2 %copy-start.7 = (bf16[96,2048]{1,0:T(8,128)(2,1)S(1)}, bf16[96,2048]{1,0:T(8,128)(2,1)}, u32[]{:S(2)}) copy-start(bf16[96,2048]{1,0:T(8,128)(2,1)} %param.27) | copy-start | bytes 1179652
  208.5 5.0 %copy-start.10 = (f32[2048]{0:T(1024)S(1)}, f32[2048]{0:T(1024)}, u32[]{:S(2)}) copy-start(f32[2048]{0:T(1024)} %param.28) | copy-start | bytes 24580
  214.5 113.4 %all-gather.14.cloned.1.call-start = ((), (), s32[]{:S(2)}) async-start(), calls=%async_computation.5 | async-start | bytes 6488064 | tf_op jit(solution)/shard_map/all_gather | solution.py:213
  215.0 206.1 %all-gather.16.cloned.1.call-start = ((), (), s32[]{:S(2)}) async-start(), calls=%async_computation.6 | async-start | bytes 6488064 | tf_op jit(solution)/shard_map/all_gather | solution.py:218
  215.6 243.1 %reduce-scatter.2.cloned.1.call-start = ((), (), s32[]{:S(2)}) async-start(), calls=%async_computation.7 | async-start | bytes 1966080 | tf_op jit(solution)/shard_map/reduce_scatter | solution.py:220
  233.5 187.6 %copy-start.12 = (bf16[384,2048]{1,0:T(8,128)(2,1)S(1)}, bf16[384,2048]{1,0:T(8,128)(2,1)}, u32[]{:S(2)}) copy-start(bf16[384,2048]{1,0:T(8,128)(2,1)} %all-gather.10.cloned.1.call-done) | copy-start | bytes 4718596
Sparse Core Ops, SparseCore 0:
  8.9 61.0 all-gather.7
  72.1 116.9 all-gather.11
  214.6 18.8 all-gather.9
  235.5 92.3 all-gather.13
  329.8 91.2 all-gather.15
  432.5 26.2 reduce-scatter.1
where the time goes:
time: 473 us; the launch traced here: 468 us
  waiting for transfers between devices  227 us (48%)
  matrix products  105 us (22%)
  blocking collectives  89.8 us (19%)
  local copies, waits for them, and re-layouts  17.1 us (4%)
  between operations  14.2 us (3%)
  other arithmetic  13.1 us (3%)
    all_gather x1, waiting for transfers between devices, per_device(): lax.all_gather(w_down, 'sp', axis=1, tiled=True)  93.2 us
    all_gather x1, waiting for transfers between devices, per_device(): lax.all_gather(w_up, 'sp', axis=0, tiled=True)  87.2 us
    all_gather x2, blocking collectives, prefix(): lax.all_gather(part.astype(kind), axis)  80 us
    reduce_scatter x1, waiting for transfers between devices, per_device(): lax.psum_scatter(channel_term.astype(jnp.bfloat16), 'tp', scatter_dimensi...  26.4 us
    all_gather x1, waiting for transfers between devices, per_device(): span_rows = lax.all_gather(normed, 'tp', axis=0, tiled=True)  17.8 us
    dot_general x1, matrix products, per_device(): jnp.dot(hidden, lax.all_gather(w_down, 'sp', axis=1, tiled=True), preferr...  11.2 us
    dot_general x8, matrix products, chain(): jnp.einsum('hkl,hlm->hkm', later[0], earlier[1], precision=EXACT_PRECISION)  10 us
    all_to_all x1, blocking collectives, per_device(): lax.all_to_all(mixed_heads, 'tp', split_axis=0, concat_axis=1, tiled=True)  9.8 us
  transfers between devices with their start and end apart: 6, of which 4 were waited for; matrix products, arithmetic and copies ran while one was open for 26% of the time, Pallas kernels for 0%

commit v1 on v0

--- a/solution.py
+++ b/solution.py
@@ -215,7 +215,9 @@
     )
     hidden = (jax.nn.silu(gate_hidden) * up_hidden).astype(jnp.bfloat16)
     channel_term = jnp.dot(
-        hidden, lax.all_gather(w_down, "sp", axis=1, tiled=True), preferred_element_type=jnp.float32
+        hidden,
+        jnp.concatenate(lax.all_gather(w_down, "sp"), axis=1),
+        preferred_element_type=jnp.float32,
     )
     channel_sum = lax.psum_scatter(
         channel_term.astype(jnp.bfloat16), "tp", scatter_dimension=0, tiled=True

time: 473 us -> 449 us (0.949)
  waiting for transfers between devices: 227 us -> 194 us
  local copies, waits for them, and re-layouts: 17.1 us -> 25.8 us
    all_gather x1, waiting for transfers between devices: 93.2 us -> 0.02 us  [per_device(): lax.all_gather(w_down, 'sp')]
    all_gather x1, waiting for transfers between devices: 0.02 us -> 58.5 us  [per_device(): lax.all_gather(w_gate, 'sp', axis=0, tiled=True)]
    reshape x0 -> x1, local copies, waits for them, and re-layouts: none -> 8.3 us  [per_device(): jnp.concatenate(lax.all_gather(w_down, 'sp'), axis=1)]
  transfers between devices with their start and end apart: 6 -> 6, of which waited for: 4 -> 4; matrix products, arithmetic and copies ran while one was open for 26% -> 29% of each run, Pallas kernels for 0% -> 0%
where the time goes in v1:
time: 449 us; the launch traced here: 444 us
  waiting for transfers between devices  194 us (43%)
  matrix products  105 us (23%)
  blocking collectives  90.3 us (20%)
  local copies, waits for them, and re-layouts  25.8 us (6%)
  between operations  14.2 us (3%)
  other arithmetic  13.3 us (3%)
    all_gather x1, waiting for transfers between devices, per_device(): lax.all_gather(w_up, 'sp', axis=0, tiled=True)  87.2 us
    all_gather x2, blocking collectives, prefix(): lax.all_gather(part.astype(kind), axis)  80.4 us
    all_gather x1, waiting for transfers between devices, per_device(): lax.all_gather(w_gate, 'sp', axis=0, tiled=True)  58.5 us
    reduce_scatter x1, waiting for transfers between devices, per_device(): lax.psum_scatter(channel_term.astype(jnp.bfloat16), 'tp', scatter_dimensi...  26.4 us
    all_gather x1, waiting for transfers between devices, per_device(): span_rows = lax.all_gather(normed, 'tp', axis=0, tiled=True)  19.3 us
    dot_general x1, matrix products, per_device(): jnp.dot(hidden, jnp.concatenate(lax.all_gather(w_down, 'sp'), axis=1), pr...  11.2 us
    dot_general x8, matrix products, chain(): jnp.einsum('hkl,hlm->hkm', later[0], earlier[1], precision=EXACT_PRECISION)  10 us
    all_to_all x1, blocking collectives, per_device(): lax.all_to_all(mixed_heads, 'tp', split_axis=0, concat_axis=1, tiled=True)  9.89 us
  transfers between devices with their start and end apart: 6, of which 4 were waited for; matrix products, arithmetic and copies ran while one was open for 29% of the time, Pallas kernels for 0%

profile of v1, /device:TPU:0, one launch (start us, length us, event | category | flops | bytes accessed | tf_op | source)
XLA Modules:
  0.0 443.8 jit_solution(16106181597497279610)
XLA Ops:
  9.0 1.8 reshape.153
  13.9 2.8 copy.77
  16.8 1.6 copy.67
  18.6 1.5 reshape.147
  20.3 6.0 %fusion.46 = (f32[6,8,64,64]{3,2,1,0:T(8,128)S(1)}, bf16[6,64,8,64]{3,1,2,0:T(8,128)(2,1)S(1)}, f32[6,8,64,64]{3,2,1,0:T(8,128)}, f32[6,8,64,64]{3,2,1,0:T(8,128)S(1)}) fusion(f32[6,8,64]{2,1,0:T(8,128)S(1)} %get-tuple-element.343, f32[6,8,64]{2,1,0:T(8,128)S(1)} %copy.69, f32[6,64,8]{1,2,0:T(8,128)S(1)} %copy.68, f32[6,64,8,64]{3,1,2,0:T(8,128)} %copy.67, ...), kind=kLoop, calls=%fused_computation.60 | loop fusion | flops 4521984 | bytes 5160960 | tf_op jit(solution)/shard_map/mul | solution.py:100
  26.3 2.7 multiply_select_fusion
  29.9 1.8 fusion.81
  31.7 1.8 fusion.82
  33.5 1.8 fusion.59
  35.3 1.8 fusion.83
  37.1 1.7 fusion.57
  38.8 1.8 fusion.84
  40.6 1.9 fusion.55
  42.5 1.8 fusion.85
  44.2 1.8 fusion.53
  46.0 1.8 fusion.51
  47.8 1.9 fusion.47
  49.6 2.2 fusion.79
  51.9 1.6 convert_multiply_fusion.1
  53.5 1.9 copy.73
  55.5 21.4 %while.43 = (s32[]{:T(128)}, f32[8,64,64]{2,1,0:T(8,128)S(1)}, f32[8,64,64]{2,1,0:T(8,128)S(1)}, f32[6,8,1]{1,2,0:T(1,128)S(1)}, f32[6,8,64,64]{2,3,1,0:T(8,128)...) while((s32[]{:T(128)}, f32[8,64,64]{2,1,0:T(8,128)S(1)}, ...), condition=%wide.region_3.4_spmd.clone.clone, body=%wide.region_2.3_spmd.clone.sunk.clone | while | flops 100802560 | bytes 2673307 | solution.py:192
  55.6 1.3 convolution_subtract_fusion.7
  57.3 1.3 convolution_add_fusion.10
  59.1 1.3 convolution_subtract_fusion.7
  60.9 1.3 convolution_add_fusion.10
  62.7 1.3 convolution_subtract_fusion.7
  64.4 1.3 convolution_add_fusion.10
  66.3 1.3 convolution_subtract_fusion.7
  68.0 1.3 convolution_add_fusion.10
  69.8 1.3 convolution_subtract_fusion.7
  71.6 1.3 convolution_add_fusion.10
  73.4 1.3 convolution_subtract_fusion.7
  75.1 1.3 convolution_add_fusion.10
  77.0 41.2 %all-gather = bf16[64,64,64]{2,1,0:T(8,128)(2,1)} all-gather(bf16[8,64,64]{2,1,0:T(8,128)(2,1)S(1)} %convert_element_type.98), channel_id=2, replica_groups=mesh['sp'=8,'tp'=4] {'sp'}, dimensions={0}, use_global_device_ids=true | all-gather | bytes 589824 | tf_op jit(solution)/shard_map/all_gather | solution.py:15
  118.1 39.2 %all-gather.1 = bf16[64,64,64]{2,1,0:T(8,128)(2,1)} all-gather(bf16[8,64,64]{2,1,0:T(8,128)(2,1)S(1)} %convert_element_type.99), channel_id=3, replica_groups=mesh['sp'=8,'tp'=4] {'sp'}, dimensions={0}, use_global_device_ids=true | all-gather | bytes 589824 | tf_op jit(solution)/shard_map/all_gather | solution.py:15
  157.4 10.7 %while.44 = (s32[]{:T(128)}, f32[8,64,64]{2,1,0:T(8,128)S(1)}, s32[]{:T(128)}, bf16[8,8,64,64]{3,2,1,0:T(8,128)(2,1)}, bf16[8,8,64,64]{3,2,1,0:T(8,128)(2,1)}) while((s32[]{:T(128)}, f32[8,64,64]{2,1,0:T(8,128)S(1)}, s32[]{:T(128)}, bf16[8,8,64,64]{3,2,1,0:T(8,128)(2,1)}, bf16[8,8,64,64]{3,2,1,0:T(8,128)(2,1)}) %tuple.113), condition=%wide.region_5.6_spmd.clone.clone, body=%wide.region_4.5_spmd.clone.sunk.clone | while | flops 25329668 | bytes 1182287 | solution.py:28
  168.1 27.8 %while.42 = (s32[]{:T(128)}, f32[8,64,64]{2,1,0:T(8,128)S(1)}, f32[6,8,64,64]{3,2,1,0:T(8,128)S(1)}, f32[6,8,1]{1,2,0:T(1,128)S(1)}, f32[6,8,64,64]{2,3,1,0:T(8,...) while((s32[]{:T(128)}, f32[8,64,64]{2,1,0:T(8,128)S(1)}, ...), condition=%wide.region_8.9_spmd.clone, body=%wide.region_7.8_spmd.sunk.clone | while | flops 100794368 | bytes 3280037 | solution.py:196
  168.1 1.4 convolution_subtract_fusion.6
  169.5 1.3 fusion.177
  170.8 1.3 fusion.178
  172.7 1.5 convolution_subtract_fusion.6
  174.2 1.3 fusion.177
  175.5 1.3 fusion.178
  177.4 1.4 convolution_subtract_fusion.6
  178.8 1.3 fusion.177
  180.1 1.3 fusion.178
  182.0 1.4 convolution_subtract_fusion.6
  183.4 1.3 fusion.177
  184.7 1.3 fusion.178
  186.6 1.4 convolution_subtract_fusion.6
  189.4 1.3 fusion.178
  191.2 1.4 convolution_subtract_fusion.6
  192.6 1.3 fusion.177
  194.0 1.3 fusion.178
  200.2 9.9 %all_to_all.19 = bf16[4,96,512]{2,1,0:T(8,128)(2,1)S(1)} all-to-all(bf16[4,96,512]{2,1,0:T(8,128)(2,1)S(1)} %bitcast.183), channel_id=1, replica_groups=mesh['sp'=8,'tp'=4] {'tp'}, dimensions={0} | all-to-all | bytes 786432 | tf_op jit(solution)/shard_map/all_to_all | solution.py:198
  210.2 5.0 %multiply_reduce_fusion.1 = (f32[96]{0:T(128)S(1)}, f32[96,2048]{1,0:T(8,128)S(1)}) fusion(bf16[96,2048]{1,0:T(8,128)(2,1)S(1)} %bitcast.179, bf16[2048,2048]{1,0:T(8,128)(2,1)} %all-gather.9.cloned.1.call-done, bf16[96,2048]{1,0:T(8,128)(2,1)S(1)} %copy-done.7), kind=kOutput, calls=%fused_computation.95 | convolution fusion | flops 806485888 | bytes 9961856 | tf_op jit(solution)/shard_map/dot_general | solution.py:200
  216.8 8.3 %copy.85 = bf16[1408,8,256]{0,2,1:T(8,128)(2,1)} copy(bf16[1408,8,256]{2,0,1:T(8,128)(2,1)} %bitcast.176) | data formatting | bytes 11534336 | tf_op jit(solution)/shard_map/reshape | solution.py:219
  225.1 58.5 %all-gather.13.cloned.1.call-done = bf16[2048,1408]{1,0:T(8,128)(2,1)} async-done(((bf16[256,1408]{1,0:T(8,128)(2,1)}), bf16[2048,1408]{1,0:T(8,128)(2,1)}) %all-gather.13.cloned.1.call-update) | async-done | bytes 5767184 | tf_op jit(solution)/shard_map/all_gather | solution.py:208
  283.6 19.3 %all-gather.11.cloned.1.call-done = bf16[384,2048]{1,0:T(8,128)(2,1)} async-done(((bf16[96,2048]{1,0:T(8,128)(2,1)}), bf16[384,2048]{1,0:T(8,128)(2,1)}) %all-gather.11.cloned.1.call-update) | async-done | bytes 1572880 | tf_op jit(solution)/shard_map/all_gather | solution.py:205
  302.9 7.2 %fusion.86 = f32[384,1408]{1,0:T(8,128)} fusion(bf16[384,2048]{1,0:T(8,128)(2,1)} %all-gather.11.cloned.1.call-done, bf16[2048,1408]{1,0:T(8,128)(2,1)} %all-gather.13.cloned.1.call-done), kind=kOutput, calls=%fused_computation.126 | convolution fusion | flops 2214592512 | bytes 9502720 | tf_op jit(solution)/shard_map/dot_general | solution.py:206
  310.0 87.2 %all-gather.15.cloned.1.call-done = bf16[2048,1408]{1,0:T(8,128)(2,1)} async-done(((bf16[256,1408]{1,0:T(8,128)(2,1)}), bf16[2048,1408]{1,0:T(8,128)(2,1)}) %all-gather.15.cloned.1.call-update) | async-done | bytes 5767184 | tf_op jit(solution)/shard_map/all_gather | solution.py:213
  397.3 11.2 %convolution_convert_fusion = bf16[384,2048]{1,0:T(8,128)(2,1)} fusion(bf16[1408,2048]{0,1:T(8,128)(2,1)} %bitcast.177, bf16[384,2048]{1,0:T(8,128)(2,1)S(1)} %copy-done.12, bf16[2048,1408]{1,0:T(8,128)(2,1)} %all-gather.15.cloned.1.call-done, f32[384,1408]{1,0:T(8,128)} %fusion.86), kind=kOutput, calls=%fused_computation.54 | convolution fusion | flops 4433215488 | bytes 16842752 | tf_op jit(solution)/shard_map/dot_general | solution.py:217
  408.5 26.4 %reduce-scatter.2.cloned.1.call-done = bf16[96,2048]{1,0:T(8,128)(2,1)} async-done(((bf16[384,2048]{1,0:T(8,128)(2,1)}), bf16[96,2048]{1,0:T(8,128)(2,1)}) %reduce-scatter.2.cloned.1.call-update) | async-done | bytes 393232 | tf_op jit(solution)/shard_map/reduce_scatter | solution.py:222
  434.9 1.8 add_convert_fusion
  (143 shorter events, 32.1 us)
Async XLA Ops:
  6.5 203.6 %all-gather.9.cloned.1.call-start = ((), (), s32[]{:S(2)}) async-start(), calls=%async_computation.2 | async-start | bytes 10485760 | tf_op jit(solution)/shard_map/all_gather | solution.py:199
  6.5 2.3 copy-start.3
  7.3 209.5 %all-gather.17.cloned.1.call-start = ((), (), s32[]{:S(2)}) async-start(), calls=%async_computation.7 | async-start | bytes 6488064 | tf_op jit(solution)/shard_map/all_gather | solution.py:219
  8.0 275.6 %all-gather.13.cloned.1.call-start = ((), (), s32[]{:S(2)}) async-start(), calls=%async_computation.4 | async-start | bytes 6488064 | tf_op jit(solution)/shard_map/all_gather | solution.py:208
  8.7 294.1 %all-gather.11.cloned.1.call-start = ((), (), s32[]{:S(2)}) async-start(), calls=%async_computation.3 | async-start | bytes 1966080 | tf_op jit(solution)/shard_map/all_gather | solution.py:205
  9.0 2.1 copy-start.4
  11.4 0.8 copy-start.8
  16.8 1.7 copy-start.9
  16.8 1.8 copy-start.5
  18.4 1.9 copy-start
  118.1 49.9 %copy-start.1 = (f32[6,8,64,64]{3,2,1,0:T(8,128)S(1)}, f32[6,8,64,64]{3,2,1,0:T(8,128)}, u32[]{:S(2)}) copy-start(f32[6,8,64,64]{3,2,1,0:T(8,128)} %custom-call.2) | copy-start | bytes 2359300
  198.5 0.7 copy-start.11
  198.5 1.2 copy-start.2
  198.5 1.4 copy-start.6
  199.9 10.2 %copy-start.7 = (bf16[96,2048]{1,0:T(8,128)(2,1)S(1)}, bf16[96,2048]{1,0:T(8,128)(2,1)}, u32[]{:S(2)}) copy-start(bf16[96,2048]{1,0:T(8,128)(2,1)} %param.27) | copy-start | bytes 1179652
  210.2 5.1 %copy-start.10 = (f32[2048]{0:T(1024)S(1)}, f32[2048]{0:T(1024)}, u32[]{:S(2)}) copy-start(f32[2048]{0:T(1024)} %param.28) | copy-start | bytes 24580
  216.1 181.1 %all-gather.15.cloned.1.call-start = ((), (), s32[]{:S(2)}) async-start(), calls=%async_computation.5 | async-start | bytes 6488064 | tf_op jit(solution)/shard_map/all_gather | solution.py:213
  216.7 218.2 %reduce-scatter.2.cloned.1.call-start = ((), (), s32[]{:S(2)}) async-start(), calls=%async_computation.6 | async-start | bytes 1966080 | tf_op jit(solution)/shard_map/reduce_scatter | solution.py:222
  302.9 94.4 %copy-start.12 = (bf16[384,2048]{1,0:T(8,128)(2,1)S(1)}, bf16[384,2048]{1,0:T(8,128)(2,1)}, u32[]{:S(2)}) copy-start(bf16[384,2048]{1,0:T(8,128)(2,1)} %all-gather.11.cloned.1.call-done) | copy-start | bytes 4718596
Sparse Core Ops, SparseCore 0:
  8.9 60.9 all-gather.8
  72.1 116.6 all-gather.16
  191.0 92.5 all-gather.12
  285.0 17.7 all-gather.10
  304.9 92.3 all-gather.14
  408.6 26.1 reduce-scatter.1
